TPU v7x, 32 devices: a whole 2x2x4 slice. The times are simulated.
32 devices in a mesh: ep: 8 (over z, core), tp: 4 (over y, x).
Axes of the slice: x: 2, y: 2, z: 4, core: 2. Of those that a mesh axis runs over, the one named last changes fastest.
Arguments:
- tokens: bfloat16 [512, 2048], P('ep', 'tp'), may hold values from -6 to 6
- gain_mix: float32 [2048], replicated, may hold values from 0.1 to 1.9
- w_in: bfloat16 [2048, 1024], P(None, 'tp'), may hold values from -0.125 to 0.125
- decay_rate: float32 [64, 64], P('tp'), may hold values from 0.05 to 3
- frequency: float32 [64, 64], P('tp'), may hold values from -3 to 3
- log_step: float32 [64], P('tp'), may hold values from -3 to 0
- input_real: float32 [64, 64, 16], P('tp'), may hold values from -1 to 1
- input_imag: float32 [64, 64, 16], P('tp'), may hold values from -1 to 1
- readout_real: float32 [64, 16, 64], P('tp'), may hold values from -0.75 to 0.75
- readout_imaginary: float32 [64, 16, 64], P('tp'), may hold values from -0.75 to 0.75
- passthrough_scale: float32 [1024], P('tp'), may hold values from -4 to 4
- state_real: float32 [512, 64, 64], P('ep', 'tp'), may hold values from -4 to 4
- state_imag: float32 [512, 64, 64], P('ep', 'tp'), may hold values from -4 to 4
- w_out: bfloat16 [1024, 2048], replicated, may hold values from -0.1875 to 0.1875
- gain_ffn: float32 [2048], replicated, may hold values from 0.1 to 1.9
- expert_choice: int32 [512, 2], P('ep'), may hold values from 0 to 7, all different within a row; in each aligned block of 64 rows (0 to 63, 64 to 127, ...) at most 32 rows name the same one
- expert_weight: float32 [512, 2], P('ep'), may hold values from 0.2 to 1
- w_gate: bfloat16 [8, 2048, 8192], P('ep', None, 'tp'), may hold values from -0.125 to 0.125
- w_up: bfloat16 [8, 2048, 8192], P('ep', None, 'tp'), may hold values from -0.125 to 0.125
- w_down: bfloat16 [8, 8192, 2048], P('ep', 'tp'), may hold values from -0.0625 to 0.0625
Outputs:
- layer_out: bfloat16 [512, 2048], P('ep', 'tp')
- next_state_real: float32 [512, 64, 64], P('ep', 'tp')
- next_state_imaginary: float32 [512, 64, 64], P('ep', 'tp')
Inputs may be any that keep to these rules, and one draw needn't show every extreme that they name: `expert_choice`: each row names 2 different experts; in the rows of one index of ep (aligned blocks of 64 rows) no expert is named more than 32 times, a bound that some block reaches.
All inputs are finite; a program needn't handle non-finite values.
Results may differ from a plain program's by a relative error of at most 0.017.
Values may be sent and summed in bfloat16 or wider, within the bound.
A program may use at most 64 MiB of HBM per device.

v0:
```python
import jax
import jax.numpy as jnp
from jax import lax
from jax.sharding import PartitionSpec as P


def state_step(
    drive,
    real_state,
    imag_state,
    decay_rate,
    frequency,
    log_step,
    input_real,
    input_imag,
    readout_real,
    readout_imaginary,
    passthrough_scale,
):
    highest_precision = lax.Precision.HIGHEST
    count_of_groups, count_of_channels = (input_real.shape[0], input_real.shape[2])
    step = jnp.exp(log_step)[:, None]
    lam_real = -decay_rate
    magnitude = jnp.exp(lam_real * step)
    abar_real = magnitude * jnp.cos(frequency * step)
    abar_imag = magnitude * jnp.sin(frequency * step)
    denom = lam_real * lam_real + frequency * frequency
    numer = abar_real - 1.0
    factor_real = (numer * lam_real + abar_imag * frequency) / denom
    factor_imag = (abar_imag * lam_real - numer * frequency) / denom
    bbar_real = factor_real[..., None] * input_real - factor_imag[..., None] * input_imag
    bbar_imag = factor_real[..., None] * input_imag + factor_imag[..., None] * input_real
    float_values = drive.astype(jnp.float32).reshape(
        drive.shape[0], count_of_groups, count_of_channels
    )
    push_real = jnp.einsum("sgc,gpc->sgp", float_values, bbar_real, precision=highest_precision)
    push_imag = jnp.einsum("sgc,gpc->sgp", float_values, bbar_imag, precision=highest_precision)
    next_state_real = abar_real * real_state - abar_imag * imag_state + push_real
    next_state_imaginary = abar_real * imag_state + abar_imag * real_state + push_imag
    readout_matrix = (
        jnp.einsum("jdr,dyr->jdy", next_state_real, readout_real, precision=highest_precision)
        - jnp.einsum(
            "jdr,dyr->jdy", next_state_imaginary, readout_imaginary, precision=highest_precision
        )
        + passthrough_scale.reshape(count_of_groups, count_of_channels) * float_values
    )
    mixer = jax.nn.gelu(
        readout_matrix.reshape(drive.shape[0], count_of_groups * count_of_channels)
    ).astype(jnp.bfloat16)
    return (mixer, next_state_real, next_state_imaginary)


def slot_table(routes, expert_count, capacity):
    flat = routes.reshape(-1)
    onehot = (flat[:, None] == jnp.arange(expert_count, dtype=jnp.int32)[None, :]).astype(jnp.int32)
    before = jnp.cumsum(onehot, axis=0) - onehot
    slot = jnp.sum(before * onehot, axis=1)
    target = flat * capacity + slot
    return (
        target[None, :] == jnp.arange(expert_count * capacity, dtype=jnp.int32)[:, None]
    ).astype(jnp.bfloat16)


def body(
    tokens,
    gain_mix,
    w_in,
    decay_rate,
    frequency,
    log_step,
    input_real,
    input_imag,
    readout_real,
    readout_imaginary,
    passthrough_scale,
    state_real,
    state_imag,
    w_out,
    gain_ffn,
    expert_choice,
    expert_weight,
    w_gate,
    w_up,
    w_down,
):
    tp_count = lax.axis_size("tp")
    expert_count = lax.axis_size("ep")
    tp_rank = lax.axis_index("tp")
    row_count, local_width = tokens.shape
    full_width = local_width * tp_count
    feature_start = tp_rank * local_width
    gain_local = lax.dynamic_slice_in_dim(gain_mix, feature_start, local_width)
    float_values = tokens.astype(jnp.float32)
    totals = lax.psum(jnp.sum(float_values * float_values, axis=1), "tp")
    scale = lax.rsqrt(totals / full_width + 1e-06)
    normed_local = (float_values * scale[:, None] * gain_local).astype(jnp.bfloat16)
    weight_rows = w_in
    drive = jnp.dot(
        lax.all_gather(normed_local, "tp", axis=1, tiled=True),
        weight_rows,
        preferred_element_type=jnp.float32,
    ).astype(jnp.bfloat16)
    mixer, next_state_real, next_state_imaginary = state_step(
        drive,
        state_real,
        state_imag,
        decay_rate,
        frequency,
        log_step,
        input_real,
        input_imag,
        readout_real,
        readout_imaginary,
        passthrough_scale,
    )
    own_columns = lax.dynamic_slice_in_dim(w_out, feature_start, local_width, 1)
    weight_rows = own_columns
    mixed = jnp.dot(
        lax.all_gather(mixer, "tp", axis=1, tiled=True),
        weight_rows,
        preferred_element_type=jnp.float32,
    ).astype(jnp.bfloat16)
    after_mix = (tokens.astype(jnp.float32) + mixed.astype(jnp.float32)).astype(jnp.bfloat16)
    after_floats = after_mix.astype(jnp.float32)
    ffn_totals = lax.psum(jnp.sum(after_floats * after_floats, axis=1), "tp")
    ffn_scale = lax.rsqrt(ffn_totals / full_width + 1e-06)
    ffn_gain_local = lax.dynamic_slice_in_dim(gain_ffn, feature_start, local_width)
    normed_ffn = (after_floats * ffn_scale[:, None] * ffn_gain_local).astype(jnp.bfloat16)
    top_count = expert_choice.shape[1]
    capacity = 2 * row_count * top_count // expert_count
    table = slot_table(expert_choice, expert_count, capacity)
    repeated = jnp.repeat(normed_ffn, top_count, axis=0)
    sent = jnp.dot(table, repeated, preferred_element_type=jnp.float32).astype(jnp.bfloat16)
    sent = sent.reshape(expert_count, capacity, local_width)
    gate_weight = w_gate[0]
    up_weight = w_up[0]
    down_weight = w_down[0]
    arrived = lax.all_to_all(sent, "ep", split_axis=0, concat_axis=0, tiled=True)
    sources, slots, _ = arrived.shape
    flat = arrived.reshape(sources * slots, local_width)
    piece = lax.all_gather(flat, "tp", axis=1, tiled=True)
    gate = jnp.dot(piece, gate_weight, preferred_element_type=jnp.float32)
    upper = jnp.dot(piece, up_weight, preferred_element_type=jnp.float32)
    hidden = (jax.nn.silu(gate) * upper).astype(jnp.bfloat16)
    partial_value = jnp.dot(hidden, down_weight, preferred_element_type=jnp.float32)
    summed = lax.psum_scatter(
        partial_value.astype(jnp.bfloat16), "tp", scatter_dimension=1, tiled=True
    )
    results = summed.reshape(sources, slots, local_width)
    returned = lax.all_to_all(results, "ep", split_axis=0, concat_axis=0, tiled=True)
    returned = returned.reshape(expert_count * capacity, local_width)
    picked = jnp.dot(table.T, returned, preferred_element_type=jnp.float32)
    picked = picked.reshape(row_count, top_count, local_width)
    weighted = jnp.sum(picked * expert_weight[..., None], axis=1)
    layer_out = (after_floats + weighted).astype(jnp.bfloat16)
    return (layer_out, next_state_real, next_state_imaginary)


def solution(mesh):
    return jax.shard_map(
        body,
        mesh=mesh,
        in_specs=(
            P("ep", "tp"),
            P(),
            P(None, "tp"),
            P("tp", None),
            P("tp", None),
            P("tp"),
            P("tp", None, None),
            P("tp", None, None),
            P("tp", None, None),
            P("tp", None, None),
            P("tp"),
            P("ep", "tp", None),
            P("ep", "tp", None),
            P(),
            P(),
            P("ep", None),
            P("ep", None),
            P("ep", None, "tp"),
            P("ep", None, "tp"),
            P("ep", "tp", None),
        ),
        out_specs=(P("ep", "tp"), P("ep", "tp", None), P("ep", "tp", None)),
        check_vma=False,
    )
```

profile of v0, /device:TPU:0, one launch (start us, length us, event | category | flops | bytes accessed | tf_op | source)
XLA Modules:
  0.0 168.3 jit_solution(3897344374055506516)
XLA Ops:
  7.3 1.0 fusion.28
  8.3 11.4 %psum.14 = f32[64]{0:T(128)S(1)} all-reduce(f32[64]{0:T(128)S(1)} %fusion.28), channel_id=1, replica_groups=mesh['ep'=8,'tp'=4] {'tp'}, use_global_device_ids=true, to_apply=%region_1.0 | all-reduce | flops 64 | bytes 512 | tf_op jit(solution)/shard_map/psum | solution.py:94
  19.7 0.8 dynamic_slice.9
  20.5 0.9 fusion.30
  21.4 8.1 %all_gather.9 = bf16[64,2048]{1,0:T(8,128)(2,1)S(1)} all-gather(bf16[64,512]{1,0:T(8,128)(2,1)S(1)} %fusion.30), channel_id=1, replica_groups=mesh['ep'=8,'tp'=4] {'tp'}, dimensions={1}, use_global_device_ids=true | all-gather | bytes 327680 | tf_op jit(solution)/shard_map/all_gather | solution.py:99
  29.5 0.3 convolution_convert_fusion.2
  29.9 0.7 exp.10
  30.6 1.3 copy.63
  31.8 1.3 copy.64
  33.1 0.8 add_divide_fusion
  34.0 0.8 fusion.16
  34.8 0.8 fusion.15
  35.7 1.5 fusion.56
  37.1 1.5 fusion.19
  38.7 9.0 %all_gather.10 = bf16[64,1024]{1,0:T(8,128)(2,1)S(1)} all-gather(bf16[64,256]{1,0:T(8,128)(2,1)S(1)} %fusion.46), channel_id=1, replica_groups=mesh['ep'=8,'tp'=4] {'tp'}, dimensions={1}, use_global_device_ids=true | all-gather | bytes 163840 | tf_op jit(solution)/shard_map/all_gather | solution.py:119
  47.7 1.6 multiply_reduce_fusion
  49.4 8.9 %psum.15 = f32[64]{0:T(128)S(1)} all-reduce(f32[64]{0:T(128)S(1)} %get-tuple-element.19), channel_id=1, replica_groups=mesh['ep'=8,'tp'=4] {'tp'}, use_global_device_ids=true, to_apply=%region_5.6 | all-reduce | flops 64 | bytes 512 | tf_op jit(solution)/shard_map/psum | solution.py:125
  58.3 0.8 dynamic_slice.11
  59.6 0.2 reduce_window_sum.11
  59.8 0.2 select_reduce_fusion
  60.0 0.2 convolution_convert_fusion
  60.2 14.5 %all_to_all.10 = bf16[8,32,512]{2,1,0:T(8,128)(2,1)} all-to-all(bf16[8,32,512]{2,1,0:T(8,128)(2,1)S(1)} %bitcast.55), channel_id=1, replica_groups=mesh['ep'=8,'tp'=4] {'ep'}, dimensions={0} | all-to-all | bytes 524288 | tf_op jit(solution)/shard_map/all_to_all | solution.py:138
  74.8 23.5 %all-gather.2.cloned.1.call-done = bf16[256,2048]{1,0:T(8,128)(2,1)} async-done(((bf16[256,512]{1,0:T(8,128)(2,1)}), bf16[256,2048]{1,0:T(8,128)(2,1)}) %all-gather.2.cloned.1.call-update) | async-done | bytes 1048592 | tf_op jit(solution)/shard_map/all_gather | solution.py:141
  98.3 7.4 %fusion.4 = f32[256,2048]{1,0:T(8,128)} fusion(bf16[256,2048]{1,0:T(8,128)(2,1)} %all-gather.2.cloned.1.call-done, bf16[1,2048,2048]{2,1,0:T(8,128)(2,1)} %param.37), kind=kOutput, calls=%fused_computation.4 | convolution fusion | flops 2147483648 | bytes 11534336 | tf_op jit(solution)/shard_map/dot_general | solution.py:142
  105.7 12.4 %fusion.12 = bf16[256,2048]{1,0:T(8,128)(2,1)} fusion(bf16[1,2048,2048]{2,1,0:T(8,128)(2,1)} %param.39, bf16[256,2048]{1,0:T(8,128)(2,1)} %all-gather.2.cloned.1.call-done, bf16[1,2048,2048]{2,1,0:T(8,128)(2,1)} %param.38, f32[256,2048]{1,0:T(8,128)} %fusion.4), kind=kOutput, calls=%fused_computation.8 | convolution fusion | flops 4298637312 | bytes 20971520 | tf_op jit(solution)/shard_map/dot_general | solution.py:145
  118.1 28.1 %reduce-scatter.2.cloned.1.call-done = bf16[256,512]{1,0:T(8,128)(2,1)} async-done(((bf16[256,2048]{1,0:T(8,128)(2,1)}), bf16[256,512]{1,0:T(8,128)(2,1)}) %reduce-scatter.2.cloned.1.call-update) | async-done | bytes 262160 | tf_op jit(solution)/shard_map/reduce_scatter | solution.py:146
  146.2 4.6 %all-to-all-start.1 = ((bf16[8,32,512]{2,1,0:T(8,128)(2,1)}), bf16[8,32,512]{2,1,0:T(8,128)(2,1)S(1)}, u32[]{:S(2)}, u32[]{:S(2)}) async-start(bf16[8,32,512]{2,1,0:T(8,128)(2,1)} %bitcast.60), calls=%async_computation.2 | async-start | bytes 524288 | tf_op jit(solution)/shard_map/all_to_all | solution.py:150
  151.0 1.0 copy.78
  152.0 1.0 copy.77
  153.1 7.4 %all-to-all-done.1 = bf16[8,32,512]{2,1,0:T(8,128)(2,1)S(1)} async-done(((bf16[8,32,512]{2,1,0:T(8,128)(2,1)}), bf16[8,32,512]{2,1,0:T(8,128)(2,1)S(1)}, u32[]{:S(2)}, u32[]{:S(2)}) %all-to-all-start.1) | async-done | bytes 262176 | tf_op jit(solution)/shard_map/all_to_all | solution.py:150
  160.6 0.2 fusion.17
  160.8 0.7 add_convert_fusion
  (34 shorter events, 1.2 us)
Async XLA Ops:
  7.2 22.3 %copy-start = (bf16[2048,256]{1,0:T(8,128)(2,1)S(1)}, bf16[2048,256]{1,0:T(8,128)(2,1)}, u32[]{:S(2)}) copy-start(bf16[2048,256]{1,0:T(8,128)(2,1)} %param.22) | copy-start | bytes 3145732
  7.2 26.8 %copy-start.3 = (f32[16,64,16]{1,2,0:T(8,128)S(1)}, f32[16,64,16]{1,2,0:T(8,128)}, u32[]{:S(2)}) copy-start(f32[16,64,16]{1,2,0:T(8,128)} %param.26) | copy-start | bytes 196612
  7.2 26.8 %copy-start.2 = (f32[16,64,16]{1,2,0:T(8,128)S(1)}, f32[16,64,16]{1,2,0:T(8,128)}, u32[]{:S(2)}) copy-start(f32[16,64,16]{1,2,0:T(8,128)} %param.27) | copy-start | bytes 196612
  7.2 28.4 %copy-start.6 = (f32[256]{0:T(256)S(1)}, f32[256]{0:T(256)}, u32[]{:S(2)}) copy-start(f32[256]{0:T(256)} %param.30) | copy-start | bytes 3076
  7.2 91.1 %all-gather.2.cloned.1.call-start = ((), (), s32[]{:S(2)}) async-start(), calls=%async_computation.3 | async-start | bytes 1310720 | tf_op jit(solution)/shard_map/all_gather | solution.py:141
  29.8 18.0 %copy-start.1 = (bf16[64,512]{1,0:T(8,128)(2,1)S(1)}, bf16[64,512]{1,0:T(8,128)(2,1)}, u32[]{:S(2)}) copy-start(bf16[64,512]{1,0:T(8,128)(2,1)} %param.20) | copy-start | bytes 196612
  33.1 26.2 %copy-start.4 = (s32[64,2]{0,1:T(2,128)S(1)}, s32[64,2]{0,1:T(2,128)}, u32[]{:S(2)}) copy-start(s32[64,2]{0,1:T(2,128)} %param.35) | copy-start | bytes 1540
  74.7 71.5 %reduce-scatter.2.cloned.1.call-start = ((), (), s32[]{:S(2)}) async-start(), calls=%async_computation.4 | async-start | bytes 1310720 | tf_op jit(solution)/shard_map/reduce_scatter | solution.py:146
  105.7 54.8 %copy-start.5 = (f32[64,2]{0,1:T(2,128)S(1)}, f32[64,2]{0,1:T(2,128)}, u32[]{:S(2)}) copy-start(f32[64,2]{0,1:T(2,128)} %param.36) | copy-start | bytes 1540
  146.2 14.3 %all-to-all-start.1 = ((bf16[8,32,512]{2,1,0:T(8,128)(2,1)}), bf16[8,32,512]{2,1,0:T(8,128)(2,1)S(1)}, u32[]{:S(2)}, u32[]{:S(2)}) async-start(bf16[8,32,512]{2,1,0:T(8,128)(2,1)} %bitcast.60), calls=%async_computation.2 | async-start | bytes 524288 | tf_op jit(solution)/shard_map/all_to_all | solution.py:150
Sparse Core Ops, SparseCore 0:
  74.9 23.4 all-gather.1
  118.3 27.9 reduce-scatter.1
where the time goes:
time: 169 us; the launch traced here: 168 us
  waiting for transfers between devices  59.1 us (35%)
  blocking collectives  51.9 us (31%)
  matrix products  26.7 us (16%)
  between operations  14.3 us (8%)
  local copies, waits for them, and re-layouts  7.69 us (5%)
  starting transfers between devices  4.69 us (3%)
  other arithmetic  4.02 us (2%)
    reduce_scatter x1, waiting for transfers between devices, body(): lax.psum_scatter(partial_value.astype(jnp.bfloat16), 'tp', scatter_dimens...  28.1 us
    all_gather x1, waiting for transfers between devices, body(): piece = lax.all_gather(flat, 'tp', axis=1, tiled=True)  23.5 us
    all_to_all x1, blocking collectives, body(): lax.all_to_all(sent, 'ep', split_axis=0, concat_axis=0, tiled=True)  14.5 us
    dot_general x1, matrix products, body(): jnp.dot(hidden, down_weight, preferred_element_type=jnp.float32)  12.4 us
    psum x1, blocking collectives, body(): totals = lax.psum(jnp.sum(float_values * float_values, axis=1), 'tp')  11.4 us
    all_gather x1, blocking collectives, body(): lax.all_gather(mixer, 'tp', axis=1, tiled=True)  8.99 us
    psum x1, blocking collectives, body(): ffn_totals = lax.psum(jnp.sum(after_floats * after_floats, axis=1), 'tp')  8.93 us
    all_gather x1, blocking collectives, body(): lax.all_gather(normed_local, 'tp', axis=1, tiled=True)  8.06 us
  transfers between devices with their start and end apart: 3, of which 3 were waited for; matrix products, arithmetic and copies ran while one was open for 1% of the time, Pallas kernels for 0%

commit v1 on v0

--- a/solution.py
+++ b/solution.py
@@ -1,6 +1,10 @@
+import functools
+
 import jax
 import jax.numpy as jnp
 from jax import lax
+from jax.experimental import pallas as pl
+from jax.experimental.pallas import tpu as pltpu
 from jax.sharding import PartitionSpec as P
 
 
@@ -61,6 +65,307 @@
     ).astype(jnp.bfloat16)
 
 
+def flipped(index, mask, count):
+    other = 0
+    bit = 1
+    while bit < count:
+        digit = lax.rem(lax.div(index, bit), 2)
+        other = other + bit * ((1 - digit) if mask & bit else digit)
+        bit *= 2
+    return other
+
+
+def expert_kernel(
+    ep_count,
+    tp_count,
+    normed_ref,
+    after_ref,
+    table_ref,
+    high_ref,
+    low_ref,
+    gate_hbm,
+    up_hbm,
+    down_hbm,
+    out_ref,
+    gate_w,
+    up_w,
+    down_w,
+    outgoing,
+    arrived,
+    gate_sum,
+    up_sum,
+    hidden,
+    parts,
+    parts_in,
+    results,
+    returned,
+    weight_sem,
+    out_send,
+    out_recv,
+    near_send,
+    near_recv,
+    far_send,
+    far_recv,
+    part_send,
+    part_recv,
+    back_send,
+    back_recv,
+):
+    me_ep, me_tp = lax.axis_index("ep"), lax.axis_index("tp")
+    capacity, width = outgoing.shape[1], outgoing.shape[2]
+    half = ep_count // 2
+    peers = sorted(range(1, tp_count), key=lambda p: (bin(p).count("1"), p))
+    near = [p for p in peers if bin(p).count("1") == 1]
+    far = [p for p in peers if p not in near]
+    tp_of = {p: flipped(me_tp, p, tp_count) for p in range(tp_count)}
+    ep_of = {j: flipped(me_ep, j, ep_count) for j in range(ep_count)}
+
+    def remote(src, dst, send, recv, **where):
+        return pltpu.make_async_remote_copy(
+            src_ref=src,
+            dst_ref=dst,
+            send_sem=send,
+            recv_sem=recv,
+            device_id=where,
+            device_id_type=pl.DeviceIdType.MESH,
+        )
+
+    order = [0] + peers
+    loads = {}
+    for p in order:
+        rows = pl.ds(pl.multiple_of(tp_of[p] * width, width), width)
+        loads[0, p] = pltpu.make_async_copy(gate_hbm.at[0, rows], gate_w.at[p], weight_sem.at[0, p])
+        loads[1, p] = pltpu.make_async_copy(up_hbm.at[0, rows], up_w.at[p], weight_sem.at[1, p])
+        loads[0, p].start()
+        loads[1, p].start()
+    down_order = far + near + [0]
+    for p in down_order:
+        columns = pl.ds(pl.multiple_of(tp_of[p] * width, width), width)
+        loads[2, p] = pltpu.make_async_copy(
+            down_hbm.at[0, :, columns], down_w.at[p], weight_sem.at[2, p]
+        )
+        loads[2, p].start()
+
+    barrier = pltpu.get_barrier_semaphore()
+    for p in peers:
+        pl.semaphore_signal(
+            barrier, inc=1, device_id={"tp": tp_of[p]}, device_id_type=pl.DeviceIdType.MESH
+        )
+    for j in range(1, ep_count):
+        pl.semaphore_signal(
+            barrier, inc=1, device_id={"ep": ep_of[j]}, device_id_type=pl.DeviceIdType.MESH
+        )
+    sent = jnp.dot(table_ref[...], normed_ref[...], preferred_element_type=jnp.float32)
+    outgoing[...] = sent.astype(jnp.bfloat16).reshape(outgoing.shape)
+    arrived[0, 0] = outgoing[me_ep]
+    pl.semaphore_wait(barrier, len(peers) + ep_count - 1)
+
+    out_copies = {}
+    for j in range(1, ep_count):
+        out_copies[j] = remote(
+            outgoing.at[ep_of[j]], arrived.at[0, j], out_send.at[j], out_recv.at[j], ep=ep_of[j]
+        )
+        out_copies[j].start()
+    near_copies, far_copies = {}, {}
+    for part in range(2):
+        for j in range(part * half, part * half + half):
+            if j:
+                out_copies[j].wait_recv()
+            for p in near:
+                near_copies[p, j] = remote(
+                    arrived.at[0, j],
+                    arrived.at[p, j],
+                    near_send.at[p, j],
+                    near_recv.at[p, j],
+                    tp=tp_of[p],
+                )
+                near_copies[p, j].start()
+        for p in far:
+            blocks = pl.ds(part * half, half)
+            far_copies[p, part] = remote(
+                arrived.at[0, blocks],
+                arrived.at[p, blocks],
+                far_send.at[p, part],
+                far_recv.at[p, part],
+                tp=tp_of[p],
+            )
+            far_copies[p, part].start()
+
+    rows = ep_count * capacity
+    hidden_width = hidden.shape[1]
+    tile = next(t for t in (512, 256, 128) if hidden_width % t == 0)
+    for place, p in enumerate(order):
+        if p in near:
+            for j in range(ep_count):
+                near_copies[p, j].wait_recv()
+        elif p:
+            for part in range(2):
+                far_copies[p, part].wait_recv()
+        loads[0, p].wait()
+        loads[1, p].wait()
+
+        @pl.loop(0, hidden_width // tile)
+        def _(n, place=place, p=p):
+            columns = pl.ds(pl.multiple_of(n * tile, tile), tile)
+            block = arrived[p].reshape(rows, width)
+            gate = jnp.dot(block, gate_w[p, :, columns], preferred_element_type=jnp.float32)
+            upper = jnp.dot(block, up_w[p, :, columns], preferred_element_type=jnp.float32)
+            if place:
+                gate = gate + gate_sum[:, columns]
+                upper = upper + up_sum[:, columns]
+            if place == len(order) - 1:
+                hidden[:, columns] = (jax.nn.silu(gate) * upper).astype(jnp.bfloat16)
+            else:
+                gate_sum[:, columns] = gate
+                up_sum[:, columns] = upper
+
+    def part_copy(p, part):
+        blocks = pl.ds((1 - part) * half * capacity, half * capacity)
+        return remote(
+            parts.at[p, blocks],
+            parts_in.at[p, blocks],
+            part_send.at[p, part],
+            part_recv.at[p, part],
+            tp=tp_of[p],
+        )
+
+    part_copies = {(p, part): part_copy(p, part) for p in peers for part in range(2)}
+    cut = next(t for t in (256, 128) if width % t == 0)
+    for p in down_order:
+        loads[2, p].wait()
+
+        @pl.loop(0, width // cut)
+        def _(n, p=p):
+            columns = pl.ds(pl.multiple_of(n * cut, cut), cut)
+            parts[p, :, columns] = jnp.dot(
+                hidden[...], down_w[p, :, columns], preferred_element_type=jnp.float32
+            ).astype(jnp.bfloat16)
+
+        if p:
+            part_copies[p, 0].start()
+        if p == down_order[-2]:
+            for q in down_order[:-1]:
+                part_copies[q, 1].start()
+
+    back_copies = {}
+    for part in range(2):
+        blocks = pl.ds((1 - part) * half * capacity, half * capacity)
+        total = None
+        for p in range(tp_count):
+            if p:
+                part_copies[p, part].wait_recv()
+                piece = parts_in[p, blocks].astype(jnp.float32)
+            else:
+                piece = parts[0, blocks].astype(jnp.float32)
+            total = piece if total is None else total + piece
+        first = (1 - part) * half
+        results[pl.ds(first, half)] = total.astype(jnp.bfloat16).reshape(half, capacity, width)
+        for j in reversed(range(first, first + half)):
+            if j:
+                back_copies[j] = remote(
+                    results.at[j],
+                    returned.at[me_ep],
+                    back_send.at[j],
+                    back_recv.at[j],
+                    ep=ep_of[j],
+                )
+                back_copies[j].start()
+    returned[me_ep] = results[0]
+    for j in range(1, ep_count):
+        remote(
+            results.at[j], returned.at[ep_of[j]], back_send.at[j], back_recv.at[j], ep=ep_of[j]
+        ).wait_recv()
+    everything = returned[...].reshape(rows, width)
+    weighted = jnp.dot(high_ref[...], everything, preferred_element_type=jnp.float32)
+    weighted = weighted + jnp.dot(low_ref[...], everything, preferred_element_type=jnp.float32)
+    out_ref[...] = (after_ref[...].astype(jnp.float32) + weighted).astype(jnp.bfloat16)
+    for copies in (out_copies, near_copies, far_copies, part_copies, back_copies):
+        for copy in copies.values():
+            copy.wait_send()
+
+
+def expert_call(normed, after, table, high, low, w_gate, w_up, w_down, ep_count, tp_count):
+    row_count, width = normed.shape
+    capacity = table.shape[0] // ep_count
+    slots = ep_count * capacity
+    hidden_width = w_gate.shape[2]
+    bf16, f32 = jnp.bfloat16, jnp.float32
+    dma = pltpu.SemaphoreType.DMA
+    vmem = pl.BlockSpec(memory_space=pltpu.VMEM)
+    hbm = pl.BlockSpec(memory_space=pl.ANY)
+    return pl.pallas_call(
+        functools.partial(expert_kernel, ep_count, tp_count),
+        out_shape=jax.ShapeDtypeStruct((row_count, width), bf16),
+        in_specs=[vmem] * 5 + [hbm] * 3,
+        out_specs=vmem,
+        scratch_shapes=[
+            pltpu.VMEM((tp_count, width, hidden_width), bf16),
+            pltpu.VMEM((tp_count, width, hidden_width), bf16),
+            pltpu.VMEM((tp_count, hidden_width, width), bf16),
+            pltpu.VMEM((ep_count, capacity, width), bf16),
+            pltpu.VMEM((tp_count, ep_count, capacity, width), bf16),
+            pltpu.VMEM((slots, hidden_width), f32),
+            pltpu.VMEM((slots, hidden_width), f32),
+            pltpu.VMEM((slots, hidden_width), bf16),
+            pltpu.VMEM((tp_count, slots, width), bf16),
+            pltpu.VMEM((tp_count, slots, width), bf16),
+            pltpu.VMEM((ep_count, capacity, width), bf16),
+            pltpu.VMEM((ep_count, capacity, width), bf16),
+            dma((3, tp_count)),
+            dma((ep_count,)),
+            dma((ep_count,)),
+            dma((tp_count, ep_count)),
+            dma((tp_count, ep_count)),
+            dma((tp_count, 2)),
+            dma((tp_count, 2)),
+            dma((tp_count, 2)),
+            dma((tp_count, 2)),
+            dma((ep_count,)),
+            dma((ep_count,)),
+        ],
+        compiler_params=pltpu.CompilerParams(
+            collective_id=0, has_side_effects=True, vmem_limit_bytes=60 * 1024 * 1024
+        ),
+    )(normed, after, table, high, low, w_gate, w_up, w_down)
+
+
+def plain_experts(normed, after, table, expert_weight, w_gate, w_up, w_down):
+    row_count, top_count = expert_weight.shape
+    expert_count = lax.axis_size("ep")
+    capacity = table.shape[0] // expert_count
+    width = normed.shape[1]
+    repeated = jnp.repeat(normed, top_count, axis=0)
+    sent = jnp.dot(table, repeated, preferred_element_type=jnp.float32).astype(jnp.bfloat16)
+    sent = sent.reshape(expert_count, capacity, width)
+    arrived = lax.all_to_all(sent, "ep", split_axis=0, concat_axis=0, tiled=True)
+    flat = arrived.reshape(expert_count * capacity, width)
+    piece = lax.all_gather(flat, "tp", axis=1, tiled=True)
+    gate = jnp.dot(piece, w_gate[0], preferred_element_type=jnp.float32)
+    upper = jnp.dot(piece, w_up[0], preferred_element_type=jnp.float32)
+    hidden = (jax.nn.silu(gate) * upper).astype(jnp.bfloat16)
+    partial_value = jnp.dot(hidden, w_down[0], preferred_element_type=jnp.float32)
+    summed = lax.psum_scatter(
+        partial_value.astype(jnp.bfloat16), "tp", scatter_dimension=1, tiled=True
+    )
+    results = summed.reshape(expert_count, capacity, width)
+    returned = lax.all_to_all(results, "ep", split_axis=0, concat_axis=0, tiled=True)
+    returned = returned.reshape(expert_count * capacity, width)
+    picked = jnp.dot(table.T, returned, preferred_element_type=jnp.float32)
+    picked = picked.reshape(row_count, top_count, width)
+    weighted = jnp.sum(picked * expert_weight[..., None], axis=1)
+    return (after.astype(jnp.float32) + weighted).astype(jnp.bfloat16)
+
+
+def norm(values, gains):
+    floats = values.astype(jnp.float32)
+    scale = lax.rsqrt(jnp.mean(floats * floats, axis=1, keepdims=True) + 1e-06)
+    return (floats * scale * gains).astype(jnp.bfloat16)
+
+
+def power_of_two(count):
+    return count & (count - 1) == 0
+
+
 def body(
     tokens,
     gain_mix,
@@ -85,20 +390,14 @@
 ):
     tp_count = lax.axis_size("tp")
     expert_count = lax.axis_size("ep")
-    tp_rank = lax.axis_index("tp")
     row_count, local_width = tokens.shape
-    full_width = local_width * tp_count
-    feature_start = tp_rank * local_width
-    gain_local = lax.dynamic_slice_in_dim(gain_mix, feature_start, local_width)
-    float_values = tokens.astype(jnp.float32)
-    totals = lax.psum(jnp.sum(float_values * float_values, axis=1), "tp")
-    scale = lax.rsqrt(totals / full_width + 1e-06)
-    normed_local = (float_values * scale[:, None] * gain_local).astype(jnp.bfloat16)
-    weight_rows = w_in
+    feature_start = lax.axis_index("tp") * local_width
+    top_count = expert_choice.shape[1]
+    capacity = 2 * row_count * top_count // expert_count
+    table = slot_table(expert_choice, expert_count, capacity)
+    all_tokens = lax.all_gather(tokens, "tp", axis=1, tiled=True)
     drive = jnp.dot(
-        lax.all_gather(normed_local, "tp", axis=1, tiled=True),
-        weight_rows,
-        preferred_element_type=jnp.float32,
+        norm(all_tokens, gain_mix), w_in, preferred_element_type=jnp.float32
     ).astype(jnp.bfloat16)
     mixer, next_state_real, next_state_imaginary = state_step(
         drive,
@@ -113,46 +412,40 @@
         readout_imaginary,
         passthrough_scale,
     )
-    own_columns = lax.dynamic_slice_in_dim(w_out, feature_start, local_width, 1)
-    weight_rows = own_columns
     mixed = jnp.dot(
-        lax.all_gather(mixer, "tp", axis=1, tiled=True),
-        weight_rows,
-        preferred_element_type=jnp.float32,
+        lax.all_gather(mixer, "tp", axis=1, tiled=True), w_out, preferred_element_type=jnp.float32
     ).astype(jnp.bfloat16)
-    after_mix = (tokens.astype(jnp.float32) + mixed.astype(jnp.float32)).astype(jnp.bfloat16)
-    after_floats = after_mix.astype(jnp.float32)
-    ffn_totals = lax.psum(jnp.sum(after_floats * after_floats, axis=1), "tp")
-    ffn_scale = lax.rsqrt(ffn_totals / full_width + 1e-06)
-    ffn_gain_local = lax.dynamic_slice_in_dim(gain_ffn, feature_start, local_width)
-    normed_ffn = (after_floats * ffn_scale[:, None] * ffn_gain_local).astype(jnp.bfloat16)
-    top_count = expert_choice.shape[1]
-    capacity = 2 * row_count * top_count // expert_count
-    table = slot_table(expert_choice, expert_count, capacity)
-    repeated = jnp.repeat(normed_ffn, top_count, axis=0)
-    sent = jnp.dot(table, repeated, preferred_element_type=jnp.float32).astype(jnp.bfloat16)
-    sent = sent.reshape(expert_count, capacity, local_width)
-    gate_weight = w_gate[0]
-    up_weight = w_up[0]
-    down_weight = w_down[0]
-    arrived = lax.all_to_all(sent, "ep", split_axis=0, concat_axis=0, tiled=True)
-    sources, slots, _ = arrived.shape
-    flat = arrived.reshape(sources * slots, local_width)
-    piece = lax.all_gather(flat, "tp", axis=1, tiled=True)
-    gate = jnp.dot(piece, gate_weight, preferred_element_type=jnp.float32)
-    upper = jnp.dot(piece, up_weight, preferred_element_type=jnp.float32)
-    hidden = (jax.nn.silu(gate) * upper).astype(jnp.bfloat16)
-    partial_value = jnp.dot(hidden, down_weight, preferred_element_type=jnp.float32)
-    summed = lax.psum_scatter(
-        partial_value.astype(jnp.bfloat16), "tp", scatter_dimension=1, tiled=True
-    )
-    results = summed.reshape(sources, slots, local_width)
-    returned = lax.all_to_all(results, "ep", split_axis=0, concat_axis=0, tiled=True)
-    returned = returned.reshape(expert_count * capacity, local_width)
-    picked = jnp.dot(table.T, returned, preferred_element_type=jnp.float32)
-    picked = picked.reshape(row_count, top_count, local_width)
-    weighted = jnp.sum(picked * expert_weight[..., None], axis=1)
-    layer_out = (after_floats + weighted).astype(jnp.bfloat16)
+    after_all = (all_tokens.astype(jnp.float32) + mixed.astype(jnp.float32)).astype(jnp.bfloat16)
+    normed_all = norm(after_all, gain_ffn)
+    after = lax.dynamic_slice_in_dim(after_all, feature_start, local_width, 1)
+    normed = lax.dynamic_slice_in_dim(normed_all, feature_start, local_width, 1)
+    if (
+        local_width % 128 == 0
+        and w_gate.shape[2] % 128 == 0
+        and capacity % 16 == 0
+        and power_of_two(tp_count)
+        and power_of_two(expert_count)
+        and 2 < tp_count <= 8
+        and 1 < expert_count <= 8
+    ):
+        pairs = table.reshape(expert_count * capacity, row_count, top_count)
+        weights = jnp.sum(pairs.astype(jnp.float32) * expert_weight[None], axis=2).T
+        high = lax.reduce_precision(weights, 8, 7)
+        low = (weights - high).astype(jnp.bfloat16)
+        layer_out = expert_call(
+            normed,
+            after,
+            jnp.sum(pairs, axis=2),
+            high.astype(jnp.bfloat16),
+            low,
+            w_gate,
+            w_up,
+            w_down,
+            expert_count,
+            tp_count,
+        )
+    else:
+        layer_out = plain_experts(normed, after, table, expert_weight, w_gate, w_up, w_down)
     return (layer_out, next_state_real, next_state_imaginary)
 
 

time: 169 us -> 85.5 us (0.51)
  waiting for transfers between devices: 59.1 us -> 0 us
  Pallas kernels: 0 us -> 42.3 us
  blocking collectives: 51.9 us -> 19.6 us
  matrix products: 26.7 us -> 9.38 us
  between operations: 14.3 us -> 0.84 us
  starting transfers between devices: 4.69 us -> 0 us
  local copies, waits for them, and re-layouts: 7.69 us -> 9.65 us
    pallas_call x0 -> x1, Pallas kernels: none -> 42.3 us  [expert_call(): pl.pallas_call(functools.partial(expert_kernel, ep_count, tp_count), out_...]
    reduce_scatter x1 -> x0, waiting for transfers between devices: 28.1 us -> none  [body(): lax.psum_scatter(partial_value.astype(jnp.bfloat16), 'tp', scatter_dimens...]
    all_gather x1 -> x0, waiting for transfers between devices: 23.5 us -> none  [body(): piece = lax.all_gather(flat, 'tp', axis=1, tiled=True)]
    psum x2 -> x0, blocking collectives: 20.3 us -> none  [the longest x1 11.4 us: body(): totals = lax.psum(jnp.sum(float_values * float_values, axis=1), 'tp')]
    dot_general x6 -> x2, matrix products: 22.2 us -> 4.08 us  [the longest x1 3.04 us: body(): jnp.dot(lax.all_gather(mixer, 'tp', axis=1, tiled=True), w_out, preferred...]
    all_to_all x1 -> x0, blocking collectives: 14.5 us -> none  [body(): lax.all_to_all(sent, 'ep', split_axis=0, concat_axis=0, tiled=True)]
    all_to_all x1 -> x0, waiting for transfers between devices: 7.43 us -> none  [body(): lax.all_to_all(results, 'ep', split_axis=0, concat_axis=0, tiled=True)]
    all_to_all x1 -> x0, starting transfers between devices: 4.61 us -> none  [body(): lax.all_to_all(results, 'ep', split_axis=0, concat_axis=0, tiled=True)]
  transfers between devices with their start and end apart: 3 -> 0, of which waited for: 3 -> 0; matrix products, arithmetic and copies ran while one was open for 1% -> 0% of each run, Pallas kernels for 0% -> 0%
where the time goes in v1:
time: 85.5 us; the launch traced here: 84.9 us
  Pallas kernels  42.3 us (49%)
  blocking collectives  19.6 us (23%)
  local copies, waits for them, and re-layouts  9.65 us (11%)
  matrix products  9.38 us (11%)
  other arithmetic  3.17 us (4%)
    pallas_call x1, Pallas kernels, expert_call(): pl.pallas_call(functools.partial(expert_kernel, ep_count, tp_count), out_...  42.3 us
    all_gather x1, blocking collectives, body(): all_tokens = lax.all_gather(tokens, 'tp', axis=1, tiled=True)  10.9 us
    all_gather x1, blocking collectives, body(): lax.all_gather(mixer, 'tp', axis=1, tiled=True)  8.68 us
    unnamed x20, local copies, waits for them, and re-layouts  6.23 us
    dot_general x1, matrix products, body(): jnp.dot(lax.all_gather(mixer, 'tp', axis=1, tiled=True), w_out, preferred...  3.04 us
    dot_general x1, matrix products, state_step(): jnp.einsum('sgc,gpc->sgp', float_values, bbar_imag, precision=highest_pre...  1.75 us

profile of v1, /device:TPU:0, one launch (start us, length us, event | category | flops | bytes accessed | tf_op | source)
XLA Modules:
  0.0 84.9 jit_solution(1299384425437132319)
XLA Ops:
  0.7 10.9 %all_gather.6 = bf16[64,2048]{1,0:T(8,128)(2,1)S(1)} all-gather(bf16[64,512]{1,0:T(8,128)(2,1)} %param.20), channel_id=1, replica_groups=mesh['ep'=8,'tp'=4] {'tp'}, dimensions={1}, use_global_device_ids=true | all-gather | bytes 327680 | tf_op jit(solution)/shard_map/all_gather | solution.py:398
  11.6 0.2 fusion.7
  11.7 1.0 %convolution_convert_fusion.1 = bf16[64,256]{1,0:T(8,128)(2,1)S(1)} fusion(bf16[2048,256]{1,0:T(8,128)(2,1)S(1)} %copy-done, bf16[64,2048]{1,0:T(8,128)(2,1)S(1)} %all_gather.6, f32[2048]{0:T(1024)} %param.21, f32[64]{0:T(128)S(1)} %add_rsqrt_fusion.1), kind=kOutput, calls=%fused_computation.11 | convolution fusion | flops 67649536 | bytes 1351936 | tf_op jit(solution)/shard_map/dot_general | solution.py:399
  12.8 0.1 copy.80
  12.9 0.7 exp.6
  13.6 0.8 add_divide_fusion
  14.4 1.3 %copy.78 = f32[64,16,64]{0,2,1:T(8,128)S(1)} copy(f32[64,16,64]{2,1,0:T(8,128)} %param.31) | data formatting | bytes 524288 | tf_op args[11]
  15.7 1.3 %copy.79 = f32[64,16,64]{0,2,1:T(8,128)S(1)} copy(f32[64,16,64]{2,1,0:T(8,128)} %param.32) | data formatting | bytes 524288 | tf_op args[12]
  17.0 0.8 fusion.4
  17.8 1.2 %fusion.38 = f32[16,64,16]{1,2,0:T(8,128)} fusion(f32[64,16,64]{0,2,1:T(8,128)S(1)} %fusion.4, f32[16,16,64]{2,1,0:T(8,128)S(1)} %copy-done.3), kind=kOutput, calls=%fused_computation.63 | convolution fusion | flops 12582912 | bytes 393216 | tf_op jit(solution)/shard_map/jdr,dyr->jdy/dot_general | solution.py:45
  19.0 1.8 %fusion.3 = f32[64,16,64]{0,2,1:T(8,128)S(1)} fusion(bf16[64,16,16]{0,2,1:T(8,128)(2,1)S(1)} %bitcast.27, f32[64,16,64]{0,2,1:T(8,128)S(1)} %copy.78, f32[64,16,64]{0,2,1:T(8,128)S(1)} %copy.79, f32[16,64]{1,0:T(8,128)S(1)} %get-tuple-element.23, f32[16,64]{1,0:T(8,128)S(1)} %get-tuple-element.21, f32[16,64,16]{1,2,0:T(8,128)} %param.26, ...), kind=kOutput, calls=%fused_computation.5 | convolution fusion | flops 12894208 | bytes 966656 | tf_op jit(solution)/shard_map/sgc,gpc->sgp/dot_general | solution.py:41
  20.9 1.5 %fusion.6 = f32[64,16,16]{0,2,1:T(8,128)S(1)} fusion(f32[16,64,16]{1,2,0:T(8,128)} %fusion.38, f32[64,16,64]{0,2,1:T(8,128)S(1)} %fusion.3, f32[16,16,64]{2,1,0:T(8,128)} %param.29, bf16[64,16,16]{0,2,1:T(8,128)(2,1)S(1)} %bitcast.28, f32[16,16]{1,0:T(8,128)S(1)} %mul.219), kind=kOutput, calls=%fused_computation.10 | convolution fusion | flops 12648448 | bytes 492544 | tf_op jit(solution)/shard_map/jdr,dyr->jdy/dot_general | solution.py:46
  22.6 8.7 %all_gather.7 = bf16[64,1024]{1,0:T(8,128)(2,1)S(1)} all-gather(bf16[64,256]{1,0:T(8,128)(2,1)S(1)} %fusion.31), channel_id=1, replica_groups=mesh['ep'=8,'tp'=4] {'tp'}, dimensions={1}, use_global_device_ids=true | all-gather | bytes 163840 | tf_op jit(solution)/shard_map/all_gather | solution.py:416
  31.2 3.0 %fusion.37 = (f32[64,2048]{1,0:T(8,128)S(1)}, bf16[64,2048]{1,0:T(8,128)(2,1)S(1)}) fusion(bf16[64,1024]{1,0:T(8,128)(2,1)S(1)} %all_gather.7, bf16[1024,2048]{1,0:T(8,128)(2,1)} %param.33, bf16[64,2048]{1,0:T(8,128)(2,1)S(1)} %all_gather.6), kind=kOutput, calls=%fused_computation.62 | convolution fusion | flops 269221888 | bytes 5373952 | tf_op jit(solution)/shard_map/dot_general | solution.py:415
  34.3 0.2 multiply_reduce_fusion
  34.5 0.8 dynamic-slice
  35.2 0.7 fusion.14.normed_ref
  35.9 0.6 constant_dynamic-slice_fusion.after_ref
  36.6 0.1 copy.90
  36.7 0.1 eq.29
  36.8 0.1 fusion.32
  36.9 0.2 reduce_window_sum.11
  37.1 0.2 select_reduce_fusion
  37.2 0.1 reduce_sum.53
  37.5 0.1 multiply_reduce_fusion.1
  37.6 0.6 fusion.23
  38.2 0.1 fusion.22
  38.3 0.7 copy.92.table_ref
  39.1 42.3 %shard_map.211 = bf16[64,512]{1,0:T(8,128)(2,1)} custom-call(bf16[64,512]{1,0:T(8,128)(2,1)} %fusion.14.normed_ref, bf16[64,512]{1,0:T(8,128)(2,1)} %constant_dynamic-slice_fusion.after_ref, bf16[256,64]{1,0:T(8,128)(2,1)} %copy.92.table_ref, bf16[64,256]{1,0:T(8,128)(2,1)} %get-tuple-element.19.high_ref, bf16[64,256]{1,0:T(8,128)(2,1)} %get-tuple-element.18.low_ref, ...), custom_call_target="tpu_custom_call" | custom-call | tf_op jit(solution)/shard_map/pallas_call | solution.py:296
  81.4 1.0 %copy.94 = f32[64,16,64]{2,1,0:T(8,128)} copy(f32[64,16,64]{0,2,1:T(8,128)S(1)} %fusion.3) | data formatting | bytes 524288
  82.4 1.0 %copy.93 = f32[64,16,64]{2,1,0:T(8,128)} copy(f32[64,16,64]{0,2,1:T(8,128)S(1)} %fusion.4) | data formatting | bytes 524288
  83.4 1.5 %copy.98 = bf16[64,512]{1,0:T(8,128)(2,1)} copy(bf16[64,512]{1,0:T(8,128)(2,1)} %shard_map.211) | data formatting | bytes 131072
  (21 shorter events, 0.3 us)
Async XLA Ops:
  0.6 11.1 %copy-start = (bf16[2048,256]{1,0:T(8,128)(2,1)S(1)}, bf16[2048,256]{1,0:T(8,128)(2,1)}, u32[]{:S(2)}) copy-start(bf16[2048,256]{1,0:T(8,128)(2,1)} %param.22) | copy-start | bytes 3145732
  0.6 16.3 %copy-start.2 = (f32[16,64,16]{1,2,0:T(8,128)S(1)}, f32[16,64,16]{1,2,0:T(8,128)}, u32[]{:S(2)}) copy-start(f32[16,64,16]{1,2,0:T(8,128)} %param.26) | copy-start | bytes 196612
  0.7 16.3 %copy-start.1 = (f32[16,64,16]{1,2,0:T(8,128)S(1)}, f32[16,64,16]{1,2,0:T(8,128)}, u32[]{:S(2)}) copy-start(f32[16,64,16]{1,2,0:T(8,128)} %param.27) | copy-start | bytes 196612
  0.7 17.1 %copy-start.3 = (f32[16,16,64]{2,1,0:T(8,128)S(1)}, f32[16,16,64]{2,1,0:T(8,128)}, u32[]{:S(2)}) copy-start(f32[16,16,64]{2,1,0:T(8,128)} %param.28) | copy-start | bytes 196612
  11.7 9.1 %copy-start.6 = (f32[256]{0:T(256)S(1)}, f32[256]{0:T(256)}, u32[]{:S(2)}) copy-start(f32[256]{0:T(256)} %param.30) | copy-start | bytes 3076
  20.8 15.8 %copy-start.4 = (s32[64,2]{0,1:T(2,128)S(1)}, s32[64,2]{0,1:T(2,128)}, u32[]{:S(2)}) copy-start(s32[64,2]{0,1:T(2,128)} %param.35) | copy-start | bytes 1540
  20.8 16.7 %copy-start.5 = (f32[64,2]{0,1:T(2,128)S(1)}, f32[64,2]{0,1:T(2,128)}, u32[]{:S(2)}) copy-start(f32[64,2]{0,1:T(2,128)} %param.36) | copy-start | bytes 1540

commit v2 on v1

--- a/solution.py
+++ b/solution.py
@@ -78,15 +78,19 @@
 def expert_kernel(
     ep_count,
     tp_count,
-    normed_ref,
-    after_ref,
-    table_ref,
-    high_ref,
-    low_ref,
+    mixer_ref,
+    tokens_ref,
+    gain_ref,
+    choice_ref,
+    weight_ref,
+    out_w_hbm,
     gate_hbm,
     up_hbm,
     down_hbm,
     out_ref,
+    mixers,
+    out_w,
+    after_buffer,
     gate_w,
     up_w,
     down_w,
@@ -99,6 +103,8 @@
     parts_in,
     results,
     returned,
+    mix_send,
+    mix_recv,
     weight_sem,
     out_send,
     out_recv,
@@ -132,6 +138,11 @@
 
     order = [0] + peers
     loads = {}
+    channels = mixer_ref.shape[1]
+    for p in order:
+        rows = pl.ds(pl.multiple_of(tp_of[p] * channels, channels), channels)
+        loads[3, p] = pltpu.make_async_copy(out_w_hbm.at[rows], out_w.at[p], weight_sem.at[3, p])
+        loads[3, p].start()
     for p in order:
         rows = pl.ds(pl.multiple_of(tp_of[p] * width, width), width)
         loads[0, p] = pltpu.make_async_copy(gate_hbm.at[0, rows], gate_w.at[p], weight_sem.at[0, p])
@@ -155,10 +166,55 @@
         pl.semaphore_signal(
             barrier, inc=1, device_id={"ep": ep_of[j]}, device_id_type=pl.DeviceIdType.MESH
         )
-    sent = jnp.dot(table_ref[...], normed_ref[...], preferred_element_type=jnp.float32)
+    mixers[0] = mixer_ref[...]
+    pl.semaphore_wait(barrier, len(peers) + ep_count - 1)
+    mix_copies = {}
+    for p in far + near:
+        mix_copies[p] = remote(
+            mixer_ref, mixers.at[p], mix_send.at[p], mix_recv.at[p], tp=tp_of[p]
+        )
+        mix_copies[p].start()
+
+    row_count, top_count = choice_ref.shape
+    choice, weight = choice_ref[...], weight_ref[...]
+    spots = lax.broadcasted_iota(jnp.int32, (row_count, ep_count * capacity), 1)
+    names = lax.broadcasted_iota(jnp.int32, (row_count, 128), 1)
+    picks = [(choice[:, k : k + 1] == names).astype(jnp.float32) for k in range(top_count)]
+    earlier = (
+        lax.broadcasted_iota(jnp.int32, (row_count, row_count), 1)
+        < lax.broadcasted_iota(jnp.int32, (row_count, row_count), 0)
+    ).astype(jnp.float32)
+    before = jnp.dot(
+        earlier.astype(jnp.bfloat16),
+        sum(picks).astype(jnp.bfloat16),
+        preferred_element_type=jnp.float32,
+    )
+    table, weights = 0.0, 0.0
+    for k in range(top_count):
+        slot = jnp.sum(before * picks[k], axis=1, keepdims=True).astype(jnp.int32)
+        hit = (choice[:, k : k + 1] * capacity + slot == spots).astype(jnp.float32)
+        table = table + hit
+        weights = weights + hit * weight[:, k : k + 1]
+        before = before + picks[k]
+    high = weights.astype(jnp.bfloat16)
+    low = (weights - high.astype(jnp.float32)).astype(jnp.bfloat16)
+
+    mixed = None
+    for p in order:
+        loads[3, p].wait()
+        if p:
+            mix_copies[p].wait_recv()
+        term = jnp.dot(mixers[p], out_w[p], preferred_element_type=jnp.float32)
+        mixed = term if mixed is None else mixed + term
+    mixed = mixed.astype(jnp.bfloat16).astype(jnp.float32)
+    after = (tokens_ref[...].astype(jnp.float32) + mixed).astype(jnp.bfloat16).astype(jnp.float32)
+    scale = lax.rsqrt(jnp.mean(after * after, axis=1, keepdims=True) + 1e-06)
+    after_buffer[...] = after
+    own = pl.ds(pl.multiple_of(me_tp * width, width), width)
+    normed = (after_buffer[:, own] * scale * gain_ref[:, own]).astype(jnp.bfloat16)
+    sent = jnp.dot(table.T.astype(jnp.bfloat16), normed, preferred_element_type=jnp.float32)
     outgoing[...] = sent.astype(jnp.bfloat16).reshape(outgoing.shape)
     arrived[0, 0] = outgoing[me_ep]
-    pl.semaphore_wait(barrier, len(peers) + ep_count - 1)
 
     out_copies = {}
     for j in range(1, ep_count):
@@ -276,17 +332,103 @@
             results.at[j], returned.at[ep_of[j]], back_send.at[j], back_recv.at[j], ep=ep_of[j]
         ).wait_recv()
     everything = returned[...].reshape(rows, width)
-    weighted = jnp.dot(high_ref[...], everything, preferred_element_type=jnp.float32)
-    weighted = weighted + jnp.dot(low_ref[...], everything, preferred_element_type=jnp.float32)
-    out_ref[...] = (after_ref[...].astype(jnp.float32) + weighted).astype(jnp.bfloat16)
-    for copies in (out_copies, near_copies, far_copies, part_copies, back_copies):
+    weighted = jnp.dot(high, everything, preferred_element_type=jnp.float32)
+    weighted = weighted + jnp.dot(low, everything, preferred_element_type=jnp.float32)
+    out_ref[...] = (after_buffer[:, own] + weighted).astype(jnp.bfloat16)
+    for copies in (mix_copies, out_copies, near_copies, far_copies, part_copies, back_copies):
         for copy in copies.values():
             copy.wait_send()
 
 
-def expert_call(normed, after, table, high, low, w_gate, w_up, w_down, ep_count, tp_count):
-    row_count, width = normed.shape
-    capacity = table.shape[0] // ep_count
+def gather_kernel(
+    tp_count,
+    tokens_ref,
+    gain_ref,
+    weight_hbm,
+    all_ref,
+    drive_ref,
+    pieces,
+    weight,
+    load_sem,
+    send_sem,
+    recv_sem,
+):
+    me_tp = lax.axis_index("tp")
+    width = tokens_ref.shape[1]
+    tp_of = {p: flipped(me_tp, p, tp_count) for p in range(tp_count)}
+    order = sorted(range(tp_count), key=lambda p: (bin(p).count("1"), p))
+    loads, copies = {}, {}
+    for p in order:
+        rows = pl.ds(pl.multiple_of(tp_of[p] * width, width), width)
+        loads[p] = pltpu.make_async_copy(weight_hbm.at[rows], weight.at[p], load_sem.at[p])
+        loads[p].start()
+    barrier = pltpu.get_barrier_semaphore()
+    for p in order[1:]:
+        pl.semaphore_signal(
+            barrier, inc=1, device_id={"tp": tp_of[p]}, device_id_type=pl.DeviceIdType.MESH
+        )
+    pl.semaphore_wait(barrier, tp_count - 1)
+    for p in order[1:]:
+        copies[p] = pltpu.make_async_remote_copy(
+            src_ref=tokens_ref,
+            dst_ref=pieces.at[p],
+            send_sem=send_sem.at[p],
+            recv_sem=recv_sem.at[p],
+            device_id={"tp": tp_of[p]},
+            device_id_type=pl.DeviceIdType.MESH,
+        )
+        copies[p].start()
+    pieces[0] = tokens_ref[...]
+    squares = 0.0
+    for p in order:
+        if p:
+            copies[p].wait_recv()
+        piece = pieces[p]
+        all_ref[:, pl.ds(pl.multiple_of(tp_of[p] * width, width), width)] = piece
+        floats = piece.astype(jnp.float32)
+        squares = squares + jnp.sum(floats * floats, axis=1, keepdims=True)
+    scale = lax.rsqrt(squares / (width * tp_count) + 1e-06)
+    drive = None
+    for p in order:
+        normed = (pieces[p].astype(jnp.float32) * scale * gain_ref[tp_of[p]]).astype(jnp.bfloat16)
+        loads[p].wait()
+        term = jnp.dot(normed, weight[p], preferred_element_type=jnp.float32)
+        drive = term if drive is None else drive + term
+    drive_ref[...] = drive.astype(jnp.bfloat16)
+    for p in order[1:]:
+        copies[p].wait_send()
+
+
+def gather_call(tokens, gain, w_in, tp_count):
+    row_count, width = tokens.shape
+    channels = w_in.shape[1]
+    dma = pltpu.SemaphoreType.DMA((tp_count,))
+    vmem = pl.BlockSpec(memory_space=pltpu.VMEM)
+    return pl.pallas_call(
+        functools.partial(gather_kernel, tp_count),
+        out_shape=(
+            jax.ShapeDtypeStruct((row_count, width * tp_count), jnp.bfloat16),
+            jax.ShapeDtypeStruct((row_count, channels), jnp.bfloat16),
+        ),
+        in_specs=[vmem, vmem, pl.BlockSpec(memory_space=pl.ANY)],
+        out_specs=(vmem, vmem),
+        scratch_shapes=[
+            pltpu.VMEM((tp_count, row_count, width), jnp.bfloat16),
+            pltpu.VMEM((tp_count, width, channels), jnp.bfloat16),
+            dma,
+            dma,
+            dma,
+        ],
+        compiler_params=pltpu.CompilerParams(collective_id=1, has_side_effects=True),
+    )(tokens, gain.reshape(tp_count, 1, width), w_in)
+
+
+def expert_call(
+    mixer, tokens, gain, choice, weight, w_out, w_gate, w_up, w_down, capacity, ep_count, tp_count
+):
+    row_count, full_width = tokens.shape
+    channels = mixer.shape[1]
+    width = full_width // tp_count
     slots = ep_count * capacity
     hidden_width = w_gate.shape[2]
     bf16, f32 = jnp.bfloat16, jnp.float32
@@ -296,9 +438,12 @@
     return pl.pallas_call(
         functools.partial(expert_kernel, ep_count, tp_count),
         out_shape=jax.ShapeDtypeStruct((row_count, width), bf16),
-        in_specs=[vmem] * 5 + [hbm] * 3,
+        in_specs=[vmem] * 5 + [hbm] * 4,
         out_specs=vmem,
         scratch_shapes=[
+            pltpu.VMEM((tp_count, row_count, channels), bf16),
+            pltpu.VMEM((tp_count, channels, full_width), bf16),
+            pltpu.VMEM((row_count, full_width), f32),
             pltpu.VMEM((tp_count, width, hidden_width), bf16),
             pltpu.VMEM((tp_count, width, hidden_width), bf16),
             pltpu.VMEM((tp_count, hidden_width, width), bf16),
@@ -311,7 +456,9 @@
             pltpu.VMEM((tp_count, slots, width), bf16),
             pltpu.VMEM((ep_count, capacity, width), bf16),
             pltpu.VMEM((ep_count, capacity, width), bf16),
-            dma((3, tp_count)),
+            dma((tp_count,)),
+            dma((tp_count,)),
+            dma((4, tp_count)),
             dma((ep_count,)),
             dma((ep_count,)),
             dma((tp_count, ep_count)),
@@ -326,7 +473,7 @@
         compiler_params=pltpu.CompilerParams(
             collective_id=0, has_side_effects=True, vmem_limit_bytes=60 * 1024 * 1024
         ),
-    )(normed, after, table, high, low, w_gate, w_up, w_down)
+    )(mixer, tokens, gain.reshape(1, full_width), choice, weight, w_out, w_gate, w_up, w_down)
 
 
 def plain_experts(normed, after, table, expert_weight, w_gate, w_up, w_down):
@@ -394,11 +541,24 @@
     feature_start = lax.axis_index("tp") * local_width
     top_count = expert_choice.shape[1]
     capacity = 2 * row_count * top_count // expert_count
-    table = slot_table(expert_choice, expert_count, capacity)
-    all_tokens = lax.all_gather(tokens, "tp", axis=1, tiled=True)
-    drive = jnp.dot(
-        norm(all_tokens, gain_mix), w_in, preferred_element_type=jnp.float32
-    ).astype(jnp.bfloat16)
+    fused = (
+        local_width % 128 == 0
+        and w_gate.shape[2] % 128 == 0
+        and capacity % 16 == 0
+        and power_of_two(tp_count)
+        and power_of_two(expert_count)
+        and 2 < tp_count <= 8
+        and 1 < expert_count <= 8
+        and w_in.shape[1] % 128 == 0
+        and row_count % 16 == 0
+    )
+    if fused:
+        all_tokens, drive = gather_call(tokens, gain_mix, w_in, tp_count)
+    else:
+        all_tokens = lax.all_gather(tokens, "tp", axis=1, tiled=True)
+        drive = jnp.dot(
+            norm(all_tokens, gain_mix), w_in, preferred_element_type=jnp.float32
+        ).astype(jnp.bfloat16)
     mixer, next_state_real, next_state_imaginary = state_step(
         drive,
         state_real,
@@ -412,6 +572,23 @@
         readout_imaginary,
         passthrough_scale,
     )
+    if fused:
+        layer_out = expert_call(
+            mixer,
+            all_tokens,
+            gain_ffn,
+            expert_choice,
+            expert_weight,
+            w_out,
+            w_gate,
+            w_up,
+            w_down,
+            capacity,
+            expert_count,
+            tp_count,
+        )
+        return (layer_out, next_state_real, next_state_imaginary)
+    table = slot_table(expert_choice, expert_count, capacity)
     mixed = jnp.dot(
         lax.all_gather(mixer, "tp", axis=1, tiled=True), w_out, preferred_element_type=jnp.float32
     ).astype(jnp.bfloat16)
@@ -419,33 +596,7 @@
     normed_all = norm(after_all, gain_ffn)
     after = lax.dynamic_slice_in_dim(after_all, feature_start, local_width, 1)
     normed = lax.dynamic_slice_in_dim(normed_all, feature_start, local_width, 1)
-    if (
-        local_width % 128 == 0
-        and w_gate.shape[2] % 128 == 0
-        and capacity % 16 == 0
-        and power_of_two(tp_count)
-        and power_of_two(expert_count)
-        and 2 < tp_count <= 8
-        and 1 < expert_count <= 8
-    ):
-        pairs = table.reshape(expert_count * capacity, row_count, top_count)
-        weights = jnp.sum(pairs.astype(jnp.float32) * expert_weight[None], axis=2).T
-        high = lax.reduce_precision(weights, 8, 7)
-        low = (weights - high).astype(jnp.bfloat16)
-        layer_out = expert_call(
-            normed,
-            after,
-            jnp.sum(pairs, axis=2),
-            high.astype(jnp.bfloat16),
-            low,
-            w_gate,
-            w_up,
-            w_down,
-            expert_count,
-            tp_count,
-        )
-    else:
-        layer_out = plain_experts(normed, after, table, expert_weight, w_gate, w_up, w_down)
+    layer_out = plain_experts(normed, after, table, expert_weight, w_gate, w_up, w_down)
     return (layer_out, next_state_real, next_state_imaginary)
 
 

time: 85.5 us -> 77.7 us (0.909)
  blocking collectives: 19.6 us -> 0 us
  Pallas kernels: 42.3 us -> 58.1 us
  matrix products: 9.38 us -> 5.55 us
  other arithmetic: 3.17 us -> 1.48 us
  local copies, waits for them, and re-layouts: 9.65 us -> 11.3 us
    all_gather x2 -> x0, blocking collectives: 19.6 us -> none  [the longest x1 10.9 us: body(): all_tokens = lax.all_gather(tokens, 'tp', axis=1, tiled=True)]
    pallas_call x0 -> x1, Pallas kernels: none -> 10.2 us  [gather_call(): pl.pallas_call(functools.partial(gather_kernel, tp_count), out_shape=(jax...]
    pallas_call x1, Pallas kernels: 42.3 us -> 48 us  [expert_call(): pl.pallas_call(functools.partial(expert_kernel, ep_count, tp_count), out_...]
    dot_general x2 -> x0, matrix products: 4.08 us -> none  [the longest x1 3.04 us: body(): jnp.dot(lax.all_gather(mixer, 'tp', axis=1, tiled=True), w_out, preferred...]
    unnamed x20 -> x9, local copies, waits for them, and re-layouts: 6.23 us -> 8.87 us
    convert_element_type x3 -> x0, other arithmetic: 1.43 us -> none  [the longest x1 0.71 us: norm(): return (floats * scale * gains).astype(jnp.bfloat16)]
    dynamic_slice x2 -> x0, local copies, waits for them, and re-layouts: 1.4 us -> none  [the longest x1 0.77 us: body(): normed = lax.dynamic_slice_in_dim(normed_all, feature_start, local_width, 1)]
    dot_general x1, matrix products: 0.79 us -> 1.76 us  [state_step(): jnp.einsum('sgc,gpc->sgp', float_values, bbar_real, precision=highest_pre...]
where the time goes in v2:
time: 77.7 us; the launch traced here: 77.1 us
  Pallas kernels  58.1 us (75%)
  local copies, waits for them, and re-layouts  11.3 us (15%)
  matrix products  5.55 us (7%)
  other arithmetic  1.48 us (2%)
    pallas_call x1, Pallas kernels, expert_call(): pl.pallas_call(functools.partial(expert_kernel, ep_count, tp_count), out_...  48 us
    pallas_call x1, Pallas kernels, gather_call(): pl.pallas_call(functools.partial(gather_kernel, tp_count), out_shape=(jax...  10.2 us
    unnamed x9, local copies, waits for them, and re-layouts  8.87 us
    dot_general x1, matrix products, state_step(): jnp.einsum('sgc,gpc->sgp', float_values, bbar_real, precision=highest_pre...  1.76 us
    dot_general x1, matrix products, state_step(): jnp.einsum('sgc,gpc->sgp', float_values, bbar_imag, precision=highest_pre...  1.76 us

profile of v2, /device:TPU:0, one launch (start us, length us, event | category | flops | bytes accessed | tf_op | source)
XLA Modules:
  0.0 77.1 jit_solution(15477642599334810338)
XLA Ops:
  0.6 0.0 copy-start
  0.6 0.7 exp.6
  1.3 0.8 mul.152
  2.1 0.8 %add_divide_fusion = (f32[16,64]{1,0:T(8,128)S(1)}, f32[16,64]{1,0:T(8,128)S(1)}, f32[16,64]{1,0:T(8,128)S(1)}, f32[16,64]{1,0:T(8,128)S(1)}) fusion(f32[16,64]{1,0:T(8,128)} %param.24, f32[16,64]{1,0:T(8,128)} %param.23, f32[16]{0:T(128)S(1)} %exp.6), kind=kLoop, calls=%fused_computation.28 | loop fusion | flops 17408 | bytes 24640 | tf_op jit(solution)/shard_map/div | solution.py:33
  2.9 1.4 %copy.49.choice_ref = s32[64,2]{1,0:T(8,128)} copy(s32[64,2]{0,1:T(2,128)} %param.35) | data formatting | bytes 1024 | tf_op args[15]
  4.3 1.4 %copy.50.weight_ref = f32[64,2]{1,0:T(8,128)} copy(f32[64,2]{0,1:T(2,128)} %param.36) | data formatting | bytes 1024 | tf_op args[16]
  5.7 10.2 %shard_map.211 = (bf16[64,2048]{1,0:T(8,128)(2,1)}, bf16[64,256]{1,0:T(8,128)(2,1)}) custom-call(bf16[64,512]{1,0:T(8,128)(2,1)} %tokens_ref.1, f32[4,1,512]{2,1,0:T(1,128)} %bitcast.26, bf16[2048,256]{1,0:T(8,128)(2,1)} %weight_hbm.1), custom_call_target="tpu_custom_call" | custom-call | tf_op jit(solution)/shard_map/pallas_call | solution.py:407
  15.9 0.9 %copy.39 = bf16[64,256]{0,1:T(8,128)(2,1)S(1)} copy(bf16[64,256]{1,0:T(8,128)(2,1)} %get-tuple-element.5) | data formatting | bytes 65536 | tf_op jit(solution)/shard_map/pallas_call | solution.py:407
  16.7 1.3 %copy.37 = f32[64,16,64]{0,2,1:T(8,128)S(1)} copy(f32[64,16,64]{2,1,0:T(8,128)} %param.31) | data formatting | bytes 524288 | tf_op args[11]
  18.0 1.3 %copy.38 = f32[64,16,64]{0,2,1:T(8,128)S(1)} copy(f32[64,16,64]{2,1,0:T(8,128)} %param.32) | data formatting | bytes 524288 | tf_op args[12]
  19.3 1.8 %fusion = f32[64,16,64]{0,2,1:T(8,128)S(1)} fusion(bf16[64,16,16]{0,2,1:T(8,128)(2,1)S(1)} %bitcast.22, f32[64,16,64]{0,2,1:T(8,128)S(1)} %copy.37, f32[64,16,64]{0,2,1:T(8,128)S(1)} %copy.38, f32[16,64]{1,0:T(8,128)S(1)} %get-tuple-element.16, f32[16,64]{1,0:T(8,128)S(1)} %get-tuple-element.14, f32[16,64,16]{1,2,0:T(8,128)} %param.26, ...), kind=kOutput, calls=%fused_computation.1 | convolution fusion | flops 12894208 | bytes 966656 | tf_op jit(solution)/shard_map/sgc,gpc->sgp/dot_general | solution.py:41
  21.1 1.8 %fusion.1 = f32[64,16,64]{0,2,1:T(8,128)S(1)} fusion(bf16[64,16,16]{0,2,1:T(8,128)(2,1)S(1)} %bitcast.23, f32[64,16,64]{0,2,1:T(8,128)S(1)} %copy.38, f32[64,16,64]{0,2,1:T(8,128)S(1)} %copy.37, f32[16,64]{1,0:T(8,128)S(1)} %get-tuple-element.16, f32[16,64]{1,0:T(8,128)S(1)} %get-tuple-element.14, f32[16,64,16]{1,2,0:T(8,128)} %param.27, ...), kind=kOutput, calls=%fused_computation.3 | convolution fusion | flops 12894208 | bytes 966656 | tf_op jit(solution)/shard_map/sgc,gpc->sgp/dot_general | solution.py:40
  22.8 0.0 copy-done
  22.8 0.6 fusion.22
  23.4 1.5 %fusion.3 = f32[64,16,16]{0,2,1:T(8,128)S(1)} fusion(f32[16,64,16]{1,2,0:T(8,128)S(1)} %fusion.22, f32[64,16,64]{0,2,1:T(8,128)S(1)} %fusion, f32[16,16,64]{2,1,0:T(8,128)} %param.29, bf16[64,16,16]{0,2,1:T(8,128)(2,1)S(1)} %bitcast.24, f32[16,16]{1,0:T(8,128)S(1)} %mul.152), kind=kOutput, calls=%fused_computation.6 | convolution fusion | flops 12648448 | bytes 492544 | tf_op jit(solution)/shard_map/jdr,dyr->jdy/dot_general | solution.py:46
  24.9 1.0 %copy.52 = f32[64,16,64]{2,1,0:T(8,128)} copy(f32[64,16,64]{0,2,1:T(8,128)S(1)} %fusion) | data formatting | bytes 524288
  25.9 0.1 copy.48
  26.0 0.6 fusion.17.mixer_ref
  26.6 48.0 %shard_map.212 = bf16[64,512]{1,0:T(8,128)(2,1)} custom-call(bf16[64,256]{1,0:T(8,128)(2,1)} %fusion.17.mixer_ref, bf16[64,2048]{1,0:T(8,128)(2,1)} %get-tuple-element.6.tokens_ref, f32[1,2048]{1,0:T(1,128)} %bitcast.27, s32[64,2]{1,0:T(8,128)} %copy.49.choice_ref, f32[64,2]{1,0:T(8,128)} %copy.50.weight_ref, bf16[1024,2048]{1,0:T(8,128)(2,1)} %out_w_hbm.1, ...), custom_call_target="tpu_custom_call" | custom-call | tf_op jit(solution)/shard_map/pallas_call | solution.py:438
  74.6 1.0 %copy.51 = f32[64,16,64]{2,1,0:T(8,128)} copy(f32[64,16,64]{0,2,1:T(8,128)S(1)} %fusion.1) | data formatting | bytes 524288
  75.7 1.5 %copy.56 = bf16[64,512]{1,0:T(8,128)(2,1)} copy(bf16[64,512]{1,0:T(8,128)(2,1)} %shard_map.212) | data formatting | bytes 131072
Async XLA Ops:
  0.6 22.2 %copy-start = (f32[16,16,64]{2,1,0:T(8,128)S(1)}, f32[16,16,64]{2,1,0:T(8,128)}, u32[]{:S(2)}) copy-start(f32[16,16,64]{2,1,0:T(8,128)} %param.28) | copy-start | bytes 196612
